TPU v7x, 32 devices: a whole 2x2x4 slice. The times are simulated.
32 devices in a mesh: grp: 2 (over y), kv: 4 (over z), tp: 4 (over x, core).
Axes of the slice: x: 2, y: 2, z: 4, core: 2. Of those that a mesh axis runs over, the one named last changes fastest.
Arguments:
- tokens: bfloat16 [256, 4096], P('grp', 'kv'), parts along dimension 0, may hold values from -36 to 36
- span_lengths: int32 [256], P(('grp', 'kv')), parts along dimension 0, may hold values from 1 to 256, 13107 in all
- block_state: float32 [256, 64, 32, 64], P(('grp', 'kv'), 'tp'), parts along dimension 0, may hold values from -96 to 96
- key_cache: bfloat16 [256, 2048, 256], P(('grp', 'kv'), 'tp'), parts along dimension 0, may hold values from -6 to 6
- value_cache: bfloat16 [256, 4096, 256], P(('grp', 'kv'), 'tp'), parts along dimension 0, may hold values from -6 to 6
- decay_cache: float32 [256, 2048, 256], P(('grp', 'kv'), 'tp'), parts along dimension 0, may hold values from -34 to 0, as said below
- attn_gain: float32 [4096], P('kv'), may hold values from 0.1 to 1.9
- query_weight: bfloat16 [4096, 2048], P('kv', 'tp'), may hold values from -0.09375 to 0.09375
- key_weight: bfloat16 [4096, 2048], P('kv', 'tp'), may hold values from -0.09375 to 0.09375
- value_weight: bfloat16 [4096, 4096], P('kv', 'tp'), may hold values from -0.09375 to 0.09375
- gate_weight: bfloat16 [4096, 4096], P('kv', 'tp'), may hold values from -0.09375 to 0.09375
- decay_matrix: bfloat16 [4096, 2048], P('kv', 'tp'), may hold values from -0.09375 to 0.09375
- decay_offset_bias: float32 [2048], P('tp'), may hold values from -1.4 to 6
- head_gain: float32 [64], replicated, may hold values from 0.1 to 1.9
- out_weight: bfloat16 [4096, 4096], P('tp', 'kv'), may hold values from -0.09375 to 0.09375
- mixer_gain: float32 [4096], P('kv'), may hold values from 0.1 to 1.9
- up_weight: bfloat16 [4096, 16384], P('kv', 'tp'), may hold values from -0.09375 to 0.09375
- down_weight: bfloat16 [16384, 4096], P('tp', 'kv'), may hold values from -0.046875 to 0.046875
Outputs:
- layer_out: bfloat16 [256, 4096], P('grp', 'kv'), parts along dimension 0
There are 2 independent parts, one for each index of `grp`. A program takes and returns all parts, laid end to end along the dimension named above; an argument that names none is the same for every part. Nothing has to cross between parts.
Inputs may be any that keep to these rules, and one draw needn't show every extreme that they name: Cached positions at index span_lengths - 1 and beyond are unused. `decay_cache`: Non-increasing along positions.
All inputs are finite; a program needn't handle non-finite values. No bound on the sum of `span_lengths` on one device may be relied on, other than what follows from the above.
Results may differ from a plain program's by a relative error of at most 0.005.
The roundings to bfloat16 on the way count: a program that leaves them out, or rounds other values in their place, can miss the bound.
Values may be sent and summed in bfloat16 or wider, within the bound.
A program may use at most 128 MiB of HBM per device.

v0:
```python
import jax
import jax.numpy as jnp
from jax import lax
from jax.sharding import PartitionSpec as P

D = 4096
KEY_WIDTH = 32
DV = 64
NORM_EPS = 1e-06
DECAY_SOFTNESS = 16.0


def shards(
    tokens,
    span_lengths,
    block_state,
    key_cache,
    value_cache,
    decay_cache,
    attn_gain,
    query_weight,
    key_weight,
    value_weight,
    gate_weight,
    decay_matrix,
    decay_offset_bias,
    head_gain,
    out_weight,
    mixer_gain,
    up_weight,
    down_weight,
):
    seq_count = block_state.shape[0]
    head_count = block_state.shape[1]
    span_size = key_cache.shape[2]
    whole_rows = tokens.astype(jnp.float32)
    square_sum = jnp.sum(whole_rows * whole_rows, axis=1)
    scaled = (whole_rows * attn_gain).astype(jnp.bfloat16)
    query_part = jnp.dot(scaled, query_weight, preferred_element_type=jnp.float32)
    key_part = jnp.dot(scaled, key_weight, preferred_element_type=jnp.float32)
    value_part = jnp.dot(scaled, value_weight, preferred_element_type=jnp.float32)
    gate_part = jnp.dot(scaled, gate_weight, preferred_element_type=jnp.float32)
    decay_part = jnp.dot(scaled, decay_matrix, preferred_element_type=jnp.float32)
    square_total = lax.psum(square_sum, "kv")
    query_sum, key_sum, value_sum, gate_sum, decay_running_sum = (
        lax.psum_scatter(query_part, "kv", scatter_dimension=0, tiled=True),
        lax.psum_scatter(key_part, "kv", scatter_dimension=0, tiled=True),
        lax.psum_scatter(value_part, "kv", scatter_dimension=0, tiled=True),
        lax.psum_scatter(gate_part, "kv", scatter_dimension=0, tiled=True),
        lax.psum_scatter(decay_part, "kv", scatter_dimension=0, tiled=True),
    )
    own_square = lax.dynamic_slice_in_dim(square_total, lax.axis_index("kv") * seq_count, seq_count)
    scale_per_row = lax.rsqrt(own_square / D + NORM_EPS)[:, None]
    query = (query_sum * scale_per_row * KEY_WIDTH ** (-0.5)).reshape(
        seq_count, head_count, KEY_WIDTH
    )
    key_new = (key_sum * scale_per_row).reshape(seq_count, head_count, KEY_WIDTH)
    value_new = (value_sum * scale_per_row).reshape(seq_count, head_count, DV)
    gate = gate_sum * scale_per_row
    logarithm_decay = (
        jax.nn.log_sigmoid(decay_running_sum * scale_per_row + decay_offset_bias) / DECAY_SOFTNESS
    )
    token_place = lax.broadcasted_iota(jnp.int32, (1, 1, span_size), 2)
    lengths_now = span_lengths[:, None, None]
    previous = jnp.sum(jnp.where(token_place == lengths_now - 2, decay_cache, 0.0), axis=-1)
    now_decay = (previous + logarithm_decay).reshape(seq_count, head_count, KEY_WIDTH)
    decays_span = decay_cache.reshape(seq_count, head_count, KEY_WIDTH, span_size)
    in_use = (token_place < lengths_now - 1)[:, :, None, :]
    factor = jnp.where(in_use, jnp.exp(now_decay[..., None] - decays_span), 0.0)
    keys_span = key_cache.reshape(seq_count, head_count, KEY_WIDTH, span_size)
    scores = jnp.sum(query[..., None] * keys_span.astype(jnp.float32) * factor, axis=2)
    scores_low = scores.astype(jnp.bfloat16)
    values_span = value_cache.reshape(seq_count, head_count, DV, span_size)
    history = jnp.einsum(
        "nhs,nhvs->nhv", scores_low, values_span, preferred_element_type=jnp.float32
    )
    carried = jnp.einsum(
        "nhc,nhcv->nhv", query * jnp.exp(now_decay), block_state, precision=lax.Precision.HIGHEST
    )
    own_term = jnp.sum(query * key_new, axis=-1, keepdims=True) * value_new
    raw = carried + history + own_term
    normed = raw * lax.rsqrt(jnp.mean(raw * raw, axis=-1, keepdims=True) + NORM_EPS) * head_gain
    mixed = (normed.reshape(seq_count, head_count * DV) * jax.nn.silu(gate)).astype(jnp.bfloat16)
    attn_terms = jnp.dot(
        lax.all_gather(mixed, "kv", axis=0, tiled=True),
        out_weight,
        preferred_element_type=jnp.float32,
    )
    attn_out = lax.psum(attn_terms, "tp")
    resid = (whole_rows + attn_out).astype(jnp.bfloat16)
    resid_rows = resid.astype(jnp.float32)
    mixer_square = jnp.sum(resid_rows * resid_rows, axis=1)
    mixer_scaled = (resid_rows * mixer_gain).astype(jnp.bfloat16)
    up_part = jnp.dot(mixer_scaled, up_weight, preferred_element_type=jnp.float32)
    up_share, square_share = (
        lax.psum_scatter(up_part, "kv", scatter_dimension=0, tiled=True),
        lax.psum_scatter(mixer_square, "kv", scatter_dimension=0, tiled=True),
    )
    hidden_share = jnp.square(
        jax.nn.relu(up_share * lax.rsqrt(square_share / D + NORM_EPS)[:, None])
    )
    hidden_share = hidden_share.astype(jnp.bfloat16)
    down_terms = jnp.dot(
        lax.all_gather(hidden_share, "kv", axis=0, tiled=True),
        down_weight,
        preferred_element_type=jnp.float32,
    )
    mixer_out = lax.psum(down_terms, "tp")
    return (resid_rows + mixer_out).astype(jnp.bfloat16)


def solution(mesh):
    placed = (
        P("grp", "kv"),
        P(("grp", "kv")),
        P(("grp", "kv"), "tp", None, None),
        P(("grp", "kv"), "tp", None),
        P(("grp", "kv"), "tp", None),
        P(("grp", "kv"), "tp", None),
        P("kv"),
        P("kv", "tp"),
        P("kv", "tp"),
        P("kv", "tp"),
        P("kv", "tp"),
        P("kv", "tp"),
        P("tp"),
        P(),
        P("tp", "kv"),
        P("kv"),
        P("kv", "tp"),
        P("tp", "kv"),
    )
    return jax.shard_map(
        shards, mesh=mesh, in_specs=placed, out_specs=P("grp", "kv"), check_vma=False
    )
```

profile of v0, /device:TPU:0, one launch (start us, length us, event | category | flops | bytes accessed | tf_op | source)
XLA Modules:
  0.0 293.3 jit_solution(13781271329002494492)
XLA Ops:
  6.5 0.0 reduce-scatter.7.cloned.1.call-start
  6.6 2.5 fusion.21
  9.1 0.0 reduce-scatter.7.cloned.1.call-update
  9.1 0.0 reduce-scatter.11.cloned.1.call-start
  9.2 2.4 fusion.17
  11.5 0.0 reduce-scatter.11.cloned.1.call-update
  11.5 0.0 reduce-scatter.9.cloned.1.call-start
  11.6 2.3 fusion.19
  13.9 0.0 reduce-scatter.9.cloned.1.call-update
  14.0 0.0 reduce-scatter.13.cloned.1.call-start
  14.0 2.2 fusion.15
  16.2 0.0 reduce-scatter.13.cloned.1.call-update
  16.2 0.0 reduce-scatter.15.cloned.1.call-start
  16.3 2.9 fusion.13
  19.2 0.0 reduce-scatter.15.cloned.1.call-update
  19.2 0.0 all-reduce.4.cloned.1.call-start
  19.2 0.1 fusion.3
  19.4 13.6 %psum.21 = f32[128]{0:T(128)S(1)} all-reduce(f32[128]{0:T(128)S(1)} %fusion.3), channel_id=1, replica_groups=mesh['grp'=2,'kv'=4,'tp'=4] {'kv'}, use_global_device_ids=true, to_apply=%region_2.0 | all-reduce | flops 128 | bytes 1024 | tf_op jit(solution)/shard_map/psum | solution.py:44
  33.0 0.1 iota_compare_fusion
  33.0 0.1 iota_compare_fusion.1
  33.1 0.1 add_rsqrt_fusion.1
  33.2 8.0 %select_reduce_fusion = f32[32,512]{1,0:T(8,128)S(1)} fusion(f32[32,512,256]{2,1,0:T(8,128)} %param.23, pred[32,256]{1,0:T(8,128)(4,1)S(1)} %iota_compare_fusion.1), kind=kLoop, calls=%fused_computation.3 | loop fusion | flops 8372224 | bytes 16850944 | tf_op jit(solution)/shard_map/reduce_sum | solution.py:65
  41.2 0.0 reduce-scatter.7.cloned.1.call-done
  41.3 11.6 %reduce-scatter.11.cloned.1.call-done = f32[32,512]{1,0:T(8,128)} async-done(((f32[128,512]{1,0:T(8,128)}), f32[32,512]{1,0:T(8,128)}) %reduce-scatter.11.cloned.1.call-update) | async-done | bytes 65552 | tf_op jit(solution)/shard_map/reduce_scatter | solution.py:47
  52.9 20.5 %reduce-scatter.9.cloned.1.call-done = f32[32,512]{1,0:T(8,128)} async-done(((f32[128,512]{1,0:T(8,128)}), f32[32,512]{1,0:T(8,128)}) %reduce-scatter.9.cloned.1.call-update) | async-done | bytes 65552 | tf_op jit(solution)/shard_map/reduce_scatter | solution.py:50
  73.5 1.0 fusion.25
  74.5 0.1 reshape.83
  74.6 0.1 reshape.82
  74.7 0.1 reshape.86
  74.8 0.1 exponential_multiply_fusion
  75.0 9.7 %fusion.1 = bf16[32,16,256]{2,1,0:T(8,128)(2,1)S(1)} fusion(f32[32,16,32]{2,1,0:T(8,128)S(1)} %reshape.83, f32[32,16,32]{2,1,0:T(8,128)S(1)} %reshape.82, pred[32,256]{1,0:T(8,128)(4,1)S(1)} %iota_compare_fusion, bf16[32,512,256]{2,1,0:T(8,128)(2,1)} %param.21, f32[32,512,256]{2,1,0:T(8,128)} %param.23), kind=kLoop, calls=%fused_computation.2 | loop fusion | flops 25034752 | bytes 25567232 | tf_op jit(solution)/shard_map/reduce_sum | solution.py:71
  84.7 10.3 %fusion.8 = f32[32,16,1,64]{3,2,1,0:T(1,128)S(1)} fusion(bf16[32,16,64,256]{3,2,1,0:T(8,128)(2,1)} %bitcast.34, bf16[32,16,256,1]{2,1,0,3:T(8,128)(2,1)S(1)} %bitcast.32), kind=kOutput, calls=%fused_computation.16 | convolution fusion | flops 16777216 | bytes 17170432 | tf_op jit(solution)/shard_map/nhs,nhvs->nhv/dot_general | solution.py:74
  94.9 9.2 %fusion.29 = f32[32,16,1,64]{3,2,1,0:T(1,128)S(1)} fusion(f32[32,16,32,1]{2,3,1,0:T(1,128)S(1)} %bitcast.31, f32[32,16,32,64]{3,2,1,0:T(8,128)} %param.20), kind=kOutput, calls=%fused_computation.49 | convolution fusion | flops 12582912 | bytes 4390912 | tf_op jit(solution)/shard_map/nhc,nhcv->nhv/dot_general | solution.py:77
  104.2 0.0 reduce-scatter.13.cloned.1.call-done
  104.2 1.0 broadcast_multiply_fusion
  105.2 0.1 reshape.87
  105.3 0.2 multiply_reduce_fusion
  105.6 0.1 multiply_multiply_fusion
  105.7 0.1 reshape.88
  105.8 12.1 %reduce-scatter.15.cloned.1.call-done = f32[32,1024]{1,0:T(8,128)} async-done(((f32[128,1024]{1,0:T(8,128)}), f32[32,1024]{1,0:T(8,128)}) %reduce-scatter.15.cloned.1.call-update) | async-done | bytes 131088 | tf_op jit(solution)/shard_map/reduce_scatter | solution.py:49
  118.0 1.0 multiply_convert_fusion.1
  119.0 13.8 %all_gather.6 = bf16[128,1024]{1,0:T(8,128)(2,1)S(1)} all-gather(bf16[32,1024]{1,0:T(8,128)(2,1)S(1)} %multiply_convert_fusion.1), channel_id=1, replica_groups=mesh['grp'=2,'kv'=4,'tp'=4] {'kv'}, dimensions={0}, use_global_device_ids=true | all-gather | bytes 327680 | tf_op jit(solution)/shard_map/all_gather | solution.py:85
  132.8 1.3 fusion.30
  134.0 0.0 all-reduce.4.cloned.1.call-update
  134.1 0.2 reduce-scatter.17.cloned.1.call-start
  134.3 31.5 %all-reduce.4.cloned.1.call-done = f32[128,1024]{1,0:T(8,128)} async-done(((f32[128,1024]{1,0:T(8,128)}), f32[128,1024]{1,0:T(8,128)}) %all-reduce.4.cloned.1.call-update) | async-done | bytes 524304 | tf_op jit(solution)/shard_map/psum | solution.py:89
  165.8 1.2 fusion.6
  167.0 0.0 copy-start.9
  167.0 6.0 %fusion.10 = f32[128,4096]{1,0:T(8,128)} fusion(bf16[1024,4096]{1,0:T(8,128)(2,1)} %param.34, bf16[128,1024]{1,0:T(8,128)(2,1)S(1)} %get-tuple-element.6, f32[1024]{0:T(1024)S(1)} %copy-done.5), kind=kOutput, calls=%fused_computation.19 | convolution fusion | flops 1074135040 | bytes 10752000 | tf_op jit(solution)/shard_map/dot_general | solution.py:94
  173.0 0.0 reduce-scatter.17.cloned.1.call-update
  173.1 0.0 all-gather.2.cloned.1.call-start
  173.1 0.6 dynamic-slice
  174.4 12.1 %all-reduce = f32[128]{0:T(128)S(1)} all-reduce(f32[128]{0:T(128)S(1)} %get-tuple-element.5), channel_id=8, replica_groups=mesh['grp'=2,'kv'=4,'tp'=4] {'kv'}, use_global_device_ids=true, to_apply=%region_14.15.clone | all-reduce | flops 128 | bytes 1024
  186.4 0.1 fusion.27
  186.5 30.4 %reduce-scatter.17.cloned.1.call-done = f32[32,4096]{1,0:T(8,128)} async-done(((f32[128,4096]{1,0:T(8,128)}), f32[32,4096]{1,0:T(8,128)}) %reduce-scatter.17.cloned.1.call-update) | async-done | bytes 524304 | tf_op jit(solution)/shard_map/reduce_scatter | solution.py:96
  217.0 1.9 multiply_convert_fusion
  218.8 0.0 all-gather.2.cloned.1.call-update
  218.9 0.0 copy-start.1
  218.9 0.0 all-reduce.6.cloned.1.call-start
  218.9 27.3 %all-gather.2.cloned.1.call-done = bf16[128,4096]{1,0:T(8,128)(2,1)} async-done(((bf16[32,4096]{1,0:T(8,128)(2,1)}), bf16[128,4096]{1,0:T(8,128)(2,1)}) %all-gather.2.cloned.1.call-update) | async-done | bytes 1048592 | tf_op jit(solution)/shard_map/all_gather | solution.py:104
  246.2 5.8 %fusion.31 = f32[128,1024]{1,0:T(8,128)} fusion(bf16[128,4096]{1,0:T(8,128)(2,1)} %all-gather.2.cloned.1.call-done, bf16[4096,1024]{1,0:T(8,128)(2,1)} %param.35), kind=kOutput, calls=%fused_computation.51 | convolution fusion | flops 1073741824 | bytes 9961472 | tf_op jit(solution)/shard_map/dot_general | solution.py:103
  252.0 0.0 all-reduce.6.cloned.1.call-update
  252.0 32.9 %all-reduce.6.cloned.1.call-done = f32[128,1024]{1,0:T(8,128)} async-done(((f32[128,1024]{1,0:T(8,128)}), f32[128,1024]{1,0:T(8,128)}) %all-reduce.6.cloned.1.call-update) | async-done | bytes 524304 | tf_op jit(solution)/shard_map/psum | solution.py:108
  284.9 1.8 fusion.7
  (20 shorter events, 0.0 us)
Async XLA Ops:
  6.5 7.5 %copy-start = (bf16[1024,1024]{1,0:T(8,128)(2,1)S(1)}, bf16[1024,1024]{1,0:T(8,128)(2,1)}, u32[]{:S(2)}) copy-start(bf16[1024,1024]{1,0:T(8,128)(2,1)} %param.27) | copy-start | bytes 6291460
  6.5 9.8 %copy-start.2 = (bf16[128,1024]{1,0:T(8,128)(2,1)S(1)}, bf16[128,1024]{1,0:T(8,128)(2,1)}, u32[]{:S(2)}) copy-start(bf16[128,1024]{1,0:T(8,128)(2,1)} %param.18) | copy-start | bytes 786436
  6.5 9.8 %copy-start.4 = (f32[1024]{0:T(1024)S(1)}, f32[1024]{0:T(1024)}, u32[]{:S(2)}) copy-start(f32[1024]{0:T(1024)} %param.24) | copy-start | bytes 12292
  6.5 26.4 %copy-start.8 = (s32[32]{0:T(128)S(1)}, s32[32]{0:T(128)}, u32[]{:S(2)}) copy-start(s32[32]{0:T(128)} %param.19) | copy-start | bytes 388
  6.5 34.7 %reduce-scatter.7.cloned.1.call-start = ((), (), s32[]{:S(2)}) async-start(), calls=%async_computation.6 | async-start | bytes 327680 | tf_op jit(solution)/shard_map/reduce_scatter | solution.py:46
  9.1 43.8 %reduce-scatter.11.cloned.1.call-start = ((), (), s32[]{:S(2)}) async-start(), calls=%async_computation.8 | async-start | bytes 327680 | tf_op jit(solution)/shard_map/reduce_scatter | solution.py:47
  11.5 61.9 %reduce-scatter.9.cloned.1.call-start = ((), (), s32[]{:S(2)}) async-start(), calls=%async_computation.7 | async-start | bytes 327680 | tf_op jit(solution)/shard_map/reduce_scatter | solution.py:50
  14.0 90.2 %reduce-scatter.13.cloned.1.call-start = ((), (), s32[]{:S(2)}) async-start(), calls=%async_computation.9 | async-start | bytes 655360 | tf_op jit(solution)/shard_map/reduce_scatter | solution.py:48
  16.2 101.7 %reduce-scatter.15.cloned.1.call-start = ((), (), s32[]{:S(2)}) async-start(), calls=%async_computation.10 | async-start | bytes 655360 | tf_op jit(solution)/shard_map/reduce_scatter | solution.py:49
  19.2 146.6 %all-reduce.4.cloned.1.call-start = ((), (), s32[]{:S(2)}) async-start(), calls=%async_computation.11 | async-start | bytes 1048576 | tf_op jit(solution)/shard_map/psum | solution.py:89
  33.2 40.2 %copy-start.6 = (f32[512]{0:T(512)S(1)}, f32[512]{0:T(512)}, u32[]{:S(2)}) copy-start(f32[512]{0:T(512)} %param.30) | copy-start | bytes 6148
  94.9 10.6 %copy-start.7 = (f32[64]{0:T(128)S(1)}, f32[64]{0:T(128)}, u32[]{:S(2)}) copy-start(f32[64]{0:T(128)} %param.31) | copy-start | bytes 772
  94.9 37.9 %copy-start.3 = (bf16[1024,1024]{1,0:T(8,128)(2,1)S(1)}, bf16[1024,1024]{1,0:T(8,128)(2,1)}, u32[]{:S(2)}) copy-start(bf16[1024,1024]{1,0:T(8,128)(2,1)} %param.32) | copy-start | bytes 6291460
  94.9 72.1 %copy-start.5 = (f32[1024]{0:T(1024)S(1)}, f32[1024]{0:T(1024)}, u32[]{:S(2)}) copy-start(f32[1024]{0:T(1024)} %param.33) | copy-start | bytes 12292
  134.1 82.9 %reduce-scatter.17.cloned.1.call-start = ((), (), s32[]{:S(2)}) async-start(), calls=%async_computation.12 | async-start | bytes 2621440 | tf_op jit(solution)/shard_map/reduce_scatter | solution.py:96
  167.0 6.1 %copy-start.9 = (u32[32]{0:T(128)S(1)}, u32[32]{0:T(128)}, u32[]{:S(2)}) copy-start(u32[32]{0:T(128)} %constant.44) | copy-start | bytes 388
  173.1 73.1 %all-gather.2.cloned.1.call-start = ((), (), s32[]{:S(2)}) async-start(), calls=%async_computation.13 | async-start | bytes 1310720 | tf_op jit(solution)/shard_map/all_gather | solution.py:104
  218.9 67.9 %copy-start.1 = (bf16[1024,1024]{1,0:T(8,128)(2,1)S(1)}, bf16[1024,1024]{1,0:T(8,128)(2,1)}, u32[]{:S(2)}) copy-start(bf16[1024,1024]{1,0:T(8,128)(2,1)} %param.27) | copy-start | bytes 6291460
  218.9 66.1 %all-reduce.6.cloned.1.call-start = ((), (), s32[]{:S(2)}) async-start(), calls=%async_computation.14 | async-start | bytes 1048576 | tf_op jit(solution)/shard_map/psum | solution.py:108
Sparse Core Ops, SparseCore 0:
  9.6 22.7 reduce-scatter.6
  34.6 18.2 reduce-scatter.10
  55.2 18.2 reduce-scatter.8
  75.6 20.1 reduce-scatter.12
  97.8 20.0 reduce-scatter.14
  134.2 31.5 all-reduce.3
  173.2 43.7 reduce-scatter.16
  219.0 27.1 all-gather.1
  252.1 32.7 all-reduce.5
where the time goes:
time: 294 us; the launch traced here: 293 us
  waiting for transfers between devices  167 us (57%)
  matrix products  44.8 us (15%)
  blocking collectives  39.5 us (13%)
  other arithmetic  26.6 us (9%)
  between operations  14 us (5%)
    psum x1, waiting for transfers between devices, shards(): mixer_out = lax.psum(down_terms, 'tp')  32.9 us
    psum x1, waiting for transfers between devices, shards(): attn_out = lax.psum(attn_terms, 'tp')  31.5 us
    reduce_scatter x1, waiting for transfers between devices, shards(): lax.psum_scatter(up_part, 'kv', scatter_dimension=0, tiled=True)  30.4 us
    all_gather x1, waiting for transfers between devices, shards(): lax.all_gather(hidden_share, 'kv', axis=0, tiled=True)  27.3 us
    reduce_scatter x1, waiting for transfers between devices, shards(): lax.psum_scatter(decay_part, 'kv', scatter_dimension=0, tiled=True)  20.5 us
    all_gather x1, blocking collectives, shards(): lax.all_gather(mixed, 'kv', axis=0, tiled=True)  13.8 us
    psum x1, blocking collectives, shards(): square_total = lax.psum(square_sum, 'kv')  13.6 us
    reduce_scatter x1, waiting for transfers between devices, shards(): lax.psum_scatter(gate_part, 'kv', scatter_dimension=0, tiled=True)  12.1 us
  transfers between devices with their start and end apart: 9, of which 7 were waited for; matrix products, arithmetic and copies ran while one was open for 17% of the time, Pallas kernels for 0%

commit v1 on v0

--- a/solution.py
+++ b/solution.py
@@ -86,7 +86,7 @@
         out_weight,
         preferred_element_type=jnp.float32,
     )
-    attn_out = lax.psum(attn_terms, "tp")
+    attn_out = jnp.sum(lax.all_gather(attn_terms, "tp"), axis=0)
     resid = (whole_rows + attn_out).astype(jnp.bfloat16)
     resid_rows = resid.astype(jnp.float32)
     mixer_square = jnp.sum(resid_rows * resid_rows, axis=1)

time: 294 us -> 284 us (0.966)
  waiting for transfers between devices: 167 us -> 156 us
    psum x1 -> x0, waiting for transfers between devices: 31.5 us -> none  [shards(): attn_out = lax.psum(attn_terms, 'tp')]
    all_gather x0 -> x1, waiting for transfers between devices: none -> 20.7 us  [shards(): attn_out = jnp.sum(lax.all_gather(attn_terms, 'tp'), axis=0)]
  transfers between devices with their start and end apart: 9 -> 9, of which waited for: 7 -> 7; matrix products, arithmetic and copies ran while one was open for 17% -> 18% of each run, Pallas kernels for 0% -> 0%
where the time goes in v1:
time: 284 us; the launch traced here: 283 us
  waiting for transfers between devices  156 us (55%)
  matrix products  44.8 us (16%)
  blocking collectives  39.5 us (14%)
  other arithmetic  27.3 us (10%)
  between operations  14.1 us (5%)
    psum x1, waiting for transfers between devices, shards(): mixer_out = lax.psum(down_terms, 'tp')  32.9 us
    reduce_scatter x1, waiting for transfers between devices, shards(): lax.psum_scatter(up_part, 'kv', scatter_dimension=0, tiled=True)  30.4 us
    all_gather x1, waiting for transfers between devices, shards(): lax.all_gather(hidden_share, 'kv', axis=0, tiled=True)  27.3 us
    all_gather x1, waiting for transfers between devices, shards(): attn_out = jnp.sum(lax.all_gather(attn_terms, 'tp'), axis=0)  20.7 us
    reduce_scatter x1, waiting for transfers between devices, shards(): lax.psum_scatter(decay_part, 'kv', scatter_dimension=0, tiled=True)  20.5 us
    all_gather x1, blocking collectives, shards(): lax.all_gather(mixed, 'kv', axis=0, tiled=True)  13.8 us
    psum x1, blocking collectives, shards(): square_total = lax.psum(square_sum, 'kv')  13.6 us
    reduce_scatter x1, waiting for transfers between devices, shards(): lax.psum_scatter(gate_part, 'kv', scatter_dimension=0, tiled=True)  12.1 us
  transfers between devices with their start and end apart: 9, of which 7 were waited for; matrix products, arithmetic and copies ran while one was open for 18% of the time, Pallas kernels for 0%

profile of v1, /device:TPU:0, one launch (start us, length us, event | category | flops | bytes accessed | tf_op | source)
XLA Modules:
  0.0 283.2 jit_solution(9817129400817437764)
XLA Ops:
  6.5 0.0 reduce-scatter.7.cloned.1.call-start
  6.6 2.5 fusion.21
  9.1 0.0 reduce-scatter.7.cloned.1.call-update
  9.1 0.0 reduce-scatter.11.cloned.1.call-start
  9.2 2.4 fusion.17
  11.5 0.0 reduce-scatter.11.cloned.1.call-update
  11.5 0.0 reduce-scatter.9.cloned.1.call-start
  11.6 2.3 fusion.19
  13.9 0.0 reduce-scatter.9.cloned.1.call-update
  14.0 0.0 reduce-scatter.13.cloned.1.call-start
  14.0 2.2 fusion.15
  16.2 0.0 reduce-scatter.13.cloned.1.call-update
  16.2 0.0 reduce-scatter.15.cloned.1.call-start
  16.3 2.9 %fusion.13 = f32[128,1024]{1,0:T(8,128)} fusion(bf16[1024,1024]{1,0:T(8,128)(2,1)} %param.28, bf16[128,1024]{1,0:T(8,128)(2,1)S(1)} %copy-done.2, f32[1024]{0:T(1024)S(1)} %copy-done.4), kind=kOutput, calls=%fused_computation.29 | convolution fusion | flops 268828672 | bytes 2887680 | tf_op jit(solution)/shard_map/dot_general | solution.py:42
  19.2 0.0 reduce-scatter.15.cloned.1.call-update
  19.2 0.0 all-gather.6.cloned.1.call-start
  19.2 0.1 fusion.3
  19.4 13.6 %psum.14 = f32[128]{0:T(128)S(1)} all-reduce(f32[128]{0:T(128)S(1)} %fusion.3), channel_id=1, replica_groups=mesh['grp'=2,'kv'=4,'tp'=4] {'kv'}, use_global_device_ids=true, to_apply=%region_2.0 | all-reduce | flops 128 | bytes 1024 | tf_op jit(solution)/shard_map/psum | solution.py:44
  33.0 0.1 iota_compare_fusion
  33.0 0.1 iota_compare_fusion.1
  33.1 0.1 add_rsqrt_fusion.1
  33.2 8.0 %select_reduce_fusion = f32[32,512]{1,0:T(8,128)S(1)} fusion(f32[32,512,256]{2,1,0:T(8,128)} %param.23, pred[32,256]{1,0:T(8,128)(4,1)S(1)} %iota_compare_fusion.1), kind=kLoop, calls=%fused_computation.3 | loop fusion | flops 8372224 | bytes 16850944 | tf_op jit(solution)/shard_map/reduce_sum | solution.py:65
  41.2 0.0 reduce-scatter.7.cloned.1.call-done
  41.3 11.6 %reduce-scatter.11.cloned.1.call-done = f32[32,512]{1,0:T(8,128)} async-done(((f32[128,512]{1,0:T(8,128)}), f32[32,512]{1,0:T(8,128)}) %reduce-scatter.11.cloned.1.call-update) | async-done | bytes 65552 | tf_op jit(solution)/shard_map/reduce_scatter | solution.py:47
  52.9 20.5 %reduce-scatter.9.cloned.1.call-done = f32[32,512]{1,0:T(8,128)} async-done(((f32[128,512]{1,0:T(8,128)}), f32[32,512]{1,0:T(8,128)}) %reduce-scatter.9.cloned.1.call-update) | async-done | bytes 65552 | tf_op jit(solution)/shard_map/reduce_scatter | solution.py:50
  73.5 1.0 fusion.25
  74.5 0.1 reshape.83
  74.6 0.1 reshape.82
  74.7 0.1 reshape.86
  74.8 0.1 exponential_multiply_fusion
  75.0 9.7 %fusion.1 = bf16[32,16,256]{2,1,0:T(8,128)(2,1)S(1)} fusion(f32[32,16,32]{2,1,0:T(8,128)S(1)} %reshape.83, f32[32,16,32]{2,1,0:T(8,128)S(1)} %reshape.82, pred[32,256]{1,0:T(8,128)(4,1)S(1)} %iota_compare_fusion, bf16[32,512,256]{2,1,0:T(8,128)(2,1)} %param.21, f32[32,512,256]{2,1,0:T(8,128)} %param.23), kind=kLoop, calls=%fused_computation.2 | loop fusion | flops 25034752 | bytes 25567232 | tf_op jit(solution)/shard_map/reduce_sum | solution.py:71
  84.7 10.3 %fusion.8 = f32[32,16,1,64]{3,2,1,0:T(1,128)S(1)} fusion(bf16[32,16,64,256]{3,2,1,0:T(8,128)(2,1)} %bitcast.36, bf16[32,16,256,1]{2,1,0,3:T(8,128)(2,1)S(1)} %bitcast.34), kind=kOutput, calls=%fused_computation.16 | convolution fusion | flops 16777216 | bytes 17170432 | tf_op jit(solution)/shard_map/nhs,nhvs->nhv/dot_general | solution.py:74
  94.9 9.2 %fusion.29 = f32[32,16,1,64]{3,2,1,0:T(1,128)S(1)} fusion(f32[32,16,32,1]{2,3,1,0:T(1,128)S(1)} %bitcast.33, f32[32,16,32,64]{3,2,1,0:T(8,128)} %param.20), kind=kOutput, calls=%fused_computation.49 | convolution fusion | flops 12582912 | bytes 4390912 | tf_op jit(solution)/shard_map/nhc,nhcv->nhv/dot_general | solution.py:77
  104.2 0.0 reduce-scatter.13.cloned.1.call-done
  104.2 1.0 broadcast_multiply_fusion
  105.2 0.1 reshape.87
  105.3 0.2 multiply_reduce_fusion
  105.6 0.1 multiply_multiply_fusion
  105.7 0.1 reshape.88
  105.8 12.1 %reduce-scatter.15.cloned.1.call-done = f32[32,1024]{1,0:T(8,128)} async-done(((f32[128,1024]{1,0:T(8,128)}), f32[32,1024]{1,0:T(8,128)}) %reduce-scatter.15.cloned.1.call-update) | async-done | bytes 131088 | tf_op jit(solution)/shard_map/reduce_scatter | solution.py:49
  118.0 1.0 multiply_convert_fusion.1
  119.0 13.8 %all_gather.12 = bf16[128,1024]{1,0:T(8,128)(2,1)S(1)} all-gather(bf16[32,1024]{1,0:T(8,128)(2,1)S(1)} %multiply_convert_fusion.1), channel_id=1, replica_groups=mesh['grp'=2,'kv'=4,'tp'=4] {'kv'}, dimensions={0}, use_global_device_ids=true | all-gather | bytes 327680 | tf_op jit(solution)/shard_map/all_gather | solution.py:85
  132.8 1.2 fusion.30
  134.0 0.0 all-gather.6.cloned.1.call-update
  134.1 0.2 reduce-scatter.17.cloned.1.call-start
  134.3 20.7 %all-gather.6.cloned.1.call-done = f32[512,1024]{1,0:T(8,128)} async-done(((f32[128,1024]{1,0:T(8,128)}), f32[512,1024]{1,0:T(8,128)}) %all-gather.6.cloned.1.call-update) | async-done | bytes 2097168 | tf_op jit(solution)/shard_map/all_gather | solution.py:89
  155.0 1.8 reduce_sum.68
  156.8 0.2 fusion.6
  156.9 0.0 copy-start.9
  156.9 6.0 %fusion.10 = f32[128,4096]{1,0:T(8,128)} fusion(bf16[1024,4096]{1,0:T(8,128)(2,1)} %param.34, bf16[128,1024]{1,0:T(8,128)(2,1)S(1)} %get-tuple-element.6, f32[1024]{0:T(1024)S(1)} %copy-done.5), kind=kOutput, calls=%fused_computation.19 | convolution fusion | flops 1074135040 | bytes 10752000 | tf_op jit(solution)/shard_map/dot_general | solution.py:94
  162.9 0.0 reduce-scatter.17.cloned.1.call-update
  163.0 0.0 all-gather.4.cloned.1.call-start
  163.0 0.6 dynamic-slice
  164.3 12.1 %all-reduce = f32[128]{0:T(128)S(1)} all-reduce(f32[128]{0:T(128)S(1)} %get-tuple-element.5), channel_id=9, replica_groups=mesh['grp'=2,'kv'=4,'tp'=4] {'kv'}, use_global_device_ids=true, to_apply=%region_14.15.clone | all-reduce | flops 128 | bytes 1024
  176.4 0.1 fusion.27
  176.5 30.4 %reduce-scatter.17.cloned.1.call-done = f32[32,4096]{1,0:T(8,128)} async-done(((f32[128,4096]{1,0:T(8,128)}), f32[32,4096]{1,0:T(8,128)}) %reduce-scatter.17.cloned.1.call-update) | async-done | bytes 524304 | tf_op jit(solution)/shard_map/reduce_scatter | solution.py:96
  206.8 1.9 multiply_convert_fusion
  208.7 0.0 all-gather.4.cloned.1.call-update
  208.7 0.0 all-reduce.3.cloned.1.call-start
  208.8 27.3 %all-gather.4.cloned.1.call-done = bf16[128,4096]{1,0:T(8,128)(2,1)} async-done(((bf16[32,4096]{1,0:T(8,128)(2,1)}), bf16[128,4096]{1,0:T(8,128)(2,1)}) %all-gather.4.cloned.1.call-update) | async-done | bytes 1048592 | tf_op jit(solution)/shard_map/all_gather | solution.py:104
  236.1 5.8 %fusion.31 = f32[128,1024]{1,0:T(8,128)} fusion(bf16[128,4096]{1,0:T(8,128)(2,1)} %all-gather.4.cloned.1.call-done, bf16[4096,1024]{1,0:T(8,128)(2,1)} %param.35), kind=kOutput, calls=%fused_computation.51 | convolution fusion | flops 1073741824 | bytes 9961472 | tf_op jit(solution)/shard_map/dot_general | solution.py:103
  241.9 0.0 all-reduce.3.cloned.1.call-update
  241.9 32.9 %all-reduce.3.cloned.1.call-done = f32[128,1024]{1,0:T(8,128)} async-done(((f32[128,1024]{1,0:T(8,128)}), f32[128,1024]{1,0:T(8,128)}) %all-reduce.3.cloned.1.call-update) | async-done | bytes 524304 | tf_op jit(solution)/shard_map/psum | solution.py:108
  274.8 1.8 fusion.7
  (21 shorter events, 0.0 us)
Async XLA Ops:
  6.5 7.5 %copy-start = (bf16[1024,1024]{1,0:T(8,128)(2,1)S(1)}, bf16[1024,1024]{1,0:T(8,128)(2,1)}, u32[]{:S(2)}) copy-start(bf16[1024,1024]{1,0:T(8,128)(2,1)} %param.27) | copy-start | bytes 6291460
  6.5 9.8 %copy-start.2 = (bf16[128,1024]{1,0:T(8,128)(2,1)S(1)}, bf16[128,1024]{1,0:T(8,128)(2,1)}, u32[]{:S(2)}) copy-start(bf16[128,1024]{1,0:T(8,128)(2,1)} %param.18) | copy-start | bytes 786436
  6.5 9.8 %copy-start.4 = (f32[1024]{0:T(1024)S(1)}, f32[1024]{0:T(1024)}, u32[]{:S(2)}) copy-start(f32[1024]{0:T(1024)} %param.24) | copy-start | bytes 12292
  6.5 26.4 %copy-start.8 = (s32[32]{0:T(128)S(1)}, s32[32]{0:T(128)}, u32[]{:S(2)}) copy-start(s32[32]{0:T(128)} %param.19) | copy-start | bytes 388
  6.5 34.7 %reduce-scatter.7.cloned.1.call-start = ((), (), s32[]{:S(2)}) async-start(), calls=%async_computation.6 | async-start | bytes 327680 | tf_op jit(solution)/shard_map/reduce_scatter | solution.py:46
  9.1 43.8 %reduce-scatter.11.cloned.1.call-start = ((), (), s32[]{:S(2)}) async-start(), calls=%async_computation.8 | async-start | bytes 327680 | tf_op jit(solution)/shard_map/reduce_scatter | solution.py:47
  11.5 61.9 %reduce-scatter.9.cloned.1.call-start = ((), (), s32[]{:S(2)}) async-start(), calls=%async_computation.7 | async-start | bytes 327680 | tf_op jit(solution)/shard_map/reduce_scatter | solution.py:50
  14.0 90.2 %reduce-scatter.13.cloned.1.call-start = ((), (), s32[]{:S(2)}) async-start(), calls=%async_computation.9 | async-start | bytes 655360 | tf_op jit(solution)/shard_map/reduce_scatter | solution.py:48
  16.2 101.7 %reduce-scatter.15.cloned.1.call-start = ((), (), s32[]{:S(2)}) async-start(), calls=%async_computation.10 | async-start | bytes 655360 | tf_op jit(solution)/shard_map/reduce_scatter | solution.py:49
  19.2 135.8 %all-gather.6.cloned.1.call-start = ((), (), s32[]{:S(2)}) async-start(), calls=%async_computation.14 | async-start | bytes 2621440 | tf_op jit(solution)/shard_map/all_gather | solution.py:89
  33.2 40.2 %copy-start.6 = (f32[512]{0:T(512)S(1)}, f32[512]{0:T(512)}, u32[]{:S(2)}) copy-start(f32[512]{0:T(512)} %param.30) | copy-start | bytes 6148
  94.9 10.6 %copy-start.7 = (f32[64]{0:T(128)S(1)}, f32[64]{0:T(128)}, u32[]{:S(2)}) copy-start(f32[64]{0:T(128)} %param.31) | copy-start | bytes 772
  94.9 37.9 %copy-start.3 = (bf16[1024,1024]{1,0:T(8,128)(2,1)S(1)}, bf16[1024,1024]{1,0:T(8,128)(2,1)}, u32[]{:S(2)}) copy-start(bf16[1024,1024]{1,0:T(8,128)(2,1)} %param.32) | copy-start | bytes 6291460
  94.9 62.0 %copy-start.5 = (f32[1024]{0:T(1024)S(1)}, f32[1024]{0:T(1024)}, u32[]{:S(2)}) copy-start(f32[1024]{0:T(1024)} %param.33) | copy-start | bytes 12292
  134.1 72.8 %reduce-scatter.17.cloned.1.call-start = ((), (), s32[]{:S(2)}) async-start(), calls=%async_computation.11 | async-start | bytes 2621440 | tf_op jit(solution)/shard_map/reduce_scatter | solution.py:96
  156.9 6.1 %copy-start.9 = (u32[32]{0:T(128)S(1)}, u32[32]{0:T(128)}, u32[]{:S(2)}) copy-start(u32[32]{0:T(128)} %constant.44) | copy-start | bytes 388
  163.0 73.1 %all-gather.4.cloned.1.call-start = ((), (), s32[]{:S(2)}) async-start(), calls=%async_computation.12 | async-start | bytes 1310720 | tf_op jit(solution)/shard_map/all_gather | solution.py:104
  208.7 67.9 %copy-start.1 = (bf16[1024,1024]{1,0:T(8,128)(2,1)S(1)}, bf16[1024,1024]{1,0:T(8,128)(2,1)}, u32[]{:S(2)}) copy-start(bf16[1024,1024]{1,0:T(8,128)(2,1)} %param.27) | copy-start | bytes 6291460
  208.7 66.1 %all-reduce.3.cloned.1.call-start = ((), (), s32[]{:S(2)}) async-start(), calls=%async_computation.13 | async-start | bytes 1048576 | tf_op jit(solution)/shard_map/psum | solution.py:108
Sparse Core Ops, SparseCore 0:
  9.6 22.7 reduce-scatter.6
  34.6 18.2 reduce-scatter.10
  55.2 18.2 reduce-scatter.8
  75.6 20.1 reduce-scatter.12
  97.8 20.0 reduce-scatter.14
  134.2 20.7 all-gather.5
  163.1 43.7 reduce-scatter.16
  208.9 27.1 all-gather.3
  242.0 32.7 all-reduce.2
